TPU v7x, 256 devices: a 2x2x32 block of a 4x8x32 slice. The times are simulated.
256 devices in a mesh: grp: 4 (over y, x), ep: 64 (over z, core).
Axes of the slice: x: 2, y: 2, z: 32, core: 2. Of those that a mesh axis runs over, the one named last changes fastest.
The devices are a block of a 4x8x32 slice.
Arguments:
- tokens: bfloat16 [8192, 2048], P(('grp', 'ep')), parts along dimension 0, may hold values from -6 to 6
- norm_gain: float32 [2048], replicated, may hold values from 0.1 to 1.9
- routing: int32 [8192, 8], P(('grp', 'ep')), parts along dimension 0, may hold values from 0 to 63, all different within a row; in each aligned block of 32 rows (0 to 31, 32 to 63, ...) at most 8 rows name the same one
- gates: float32 [8192, 8], P(('grp', 'ep')), parts along dimension 0, may hold values from 0.05 to 0.6
- w_gate: bfloat16 [64, 2048, 512], P('ep'), may hold values from -0.125 to 0.125
- w_up: bfloat16 [64, 2048, 512], P('ep'), may hold values from -0.125 to 0.125
- w_down: bfloat16 [64, 512, 2048], P('ep'), may hold values from -0.25 to 0.25
- shared_gate: bfloat16 [2048, 512], replicated, may hold values from -0.125 to 0.125
- shared_up: bfloat16 [2048, 512], replicated, may hold values from -0.125 to 0.125
- shared_down: bfloat16 [512, 2048], replicated, may hold values from -0.25 to 0.25
Outputs:
- mixed: bfloat16 [8192, 2048], P(('grp', 'ep')), parts along dimension 0
There are 4 independent parts, one for each index of `grp`. A program takes and returns all parts, laid end to end along the dimension named above; an argument that names none is the same for every part. Nothing has to cross between parts.
Inputs may be any that keep to these rules, and one draw needn't show every extreme that they name: `routing`: within the 32 rows of one device no expert is named by more than 8 rows, and in every draw some expert is named by exactly 8 rows of some device; each row names 8 different experts.
All inputs are finite; a program needn't handle non-finite values.
Results may differ from a plain program's by a relative error of at most 0.0067.
Values may be sent and summed in bfloat16 or wider, within the bound.
A program may use at most 128 MiB of HBM per device.

v0:
```python
import jax
import jax.numpy as jnp
from jax import lax
from jax.sharding import PartitionSpec as P

epsilon = 1e-06


def rms_normed(tokens, norm_gain):
    floats = tokens.astype(jnp.float32)
    scale_inv = lax.rsqrt(jnp.mean(floats * floats, axis=-1, keepdims=True) + epsilon)
    return (floats * scale_inv * norm_gain).astype(jnp.bfloat16)


def body(
    tokens, norm_gain, routing, gates, w_gate, w_up, w_down, shared_gate, shared_up, shared_down
):
    normed = rms_normed(tokens, norm_gain)
    shared_hidden = (
        jax.nn.silu(jnp.dot(normed, shared_gate, preferred_element_type=jnp.float32))
        * jnp.dot(normed, shared_up, preferred_element_type=jnp.float32)
    ).astype(jnp.bfloat16)
    shared_out = jnp.dot(shared_hidden, shared_down, preferred_element_type=jnp.float32)
    everyone = lax.all_gather(normed, "ep", axis=0, tiled=True)
    routes = lax.all_gather(routing, "ep", axis=0, tiled=True)
    weights = lax.all_gather(gates, "ep", axis=0, tiled=True)
    own = lax.axis_index("ep")
    scale = jnp.sum(jnp.where(routes == own, weights, 0.0), axis=-1, keepdims=True)
    hidden = (
        jax.nn.silu(jnp.dot(everyone, w_gate[0], preferred_element_type=jnp.float32))
        * jnp.dot(everyone, w_up[0], preferred_element_type=jnp.float32)
        * scale
    )
    part = jnp.dot(
        hidden.astype(jnp.bfloat16), w_down[0], preferred_element_type=jnp.float32
    ).astype(jnp.bfloat16)
    routed = lax.psum_scatter(part, "ep", scatter_dimension=0, tiled=True)
    return (shared_out + routed.astype(jnp.float32)).astype(jnp.bfloat16)


def solution(mesh):
    placed = (
        P(("grp", "ep"), None),
        P(),
        P(("grp", "ep"), None),
        P(("grp", "ep"), None),
        P("ep", None, None),
        P("ep", None, None),
        P("ep", None, None),
        P(),
        P(),
        P(),
    )
    return jax.shard_map(
        body, mesh=mesh, in_specs=placed, out_specs=P(("grp", "ep"), None), check_vma=False
    )
```

profile of v0, /device:TPU:38, one launch (start us, length us, event | category | flops | bytes accessed | tf_op | source)
XLA Modules:
  0.0 402.0 jit_solution(2111920116285077826)
XLA Ops:
  6.5 0.0 copy-start
  6.6 0.0 all-gather.4.cloned.1.call-start
  6.6 1.2 fusion.6
  7.7 1.7 fusion.8
  9.4 0.1 all-gather.4.cloned.1.call-update
  9.5 0.1 reduce-scatter.2.cloned.1.call-start
  9.6 76.1 %all-gather = s32[64,32,8]{1,2,0:T(8,128)S(1)} all-gather(s32[1,32,8]{1,2,0:T(8,128)} %bitcast.19), channel_id=1, replica_groups=mesh['grp'=4,'ep'=64] {'ep'}, dimensions={0}, use_global_device_ids=true | all-gather | bytes 66560 | tf_op jit(solution)/shard_map/all_gather | solution.py:25
  85.6 53.4 %all-gather.1 = f32[64,32,8]{1,2,0:T(8,128)S(1)} all-gather(f32[1,32,8]{1,2,0:T(8,128)} %bitcast.20), channel_id=1, replica_groups=mesh['grp'=4,'ep'=64] {'ep'}, dimensions={0}, use_global_device_ids=true | all-gather | bytes 66560 | tf_op jit(solution)/shard_map/all_gather | solution.py:26
  139.0 0.1 select_reduce_fusion
  139.1 0.1 reshape.18
  139.2 20.5 %all-gather.4.cloned.1.call-done = bf16[2048,2048]{1,0:T(8,128)(2,1)} async-done(((bf16[32,2048]{1,0:T(8,128)(2,1)}), bf16[2048,2048]{1,0:T(8,128)(2,1)}) %all-gather.4.cloned.1.call-update) | async-done | bytes 8388624 | tf_op jit(solution)/shard_map/all_gather | solution.py:24
  159.7 0.0 copy-start.2
  159.7 0.0 copy-start.3
  159.7 7.7 %fusion.3 = f32[2048,512]{1,0:T(8,128)S(1)} fusion(bf16[2048,2048]{1,0:T(8,128)(2,1)} %all-gather.4.cloned.1.call-done, bf16[1,2048,512]{2,1,0:T(8,128)(2,1)} %param.14), kind=kOutput, calls=%fused_computation.6 | convolution fusion | flops 4294967296 | bytes 14680064 | tf_op jit(solution)/shard_map/dot_general | solution.py:30
  167.4 0.0 copy-done.2
  167.4 0.0 copy-done.3
  167.4 5.2 %multiply_convert_fusion = bf16[2048,512]{1,0:T(8,128)(2,1)S(1)} fusion(f32[2048,512]{1,0:T(8,128)S(1)} %fusion.3, bf16[2048,2048]{1,0:T(8,128)(2,1)S(1)} %copy-done.2, bf16[1,2048,512]{2,1,0:T(8,128)(2,1)S(1)} %copy-done.3, f32[2048]{0:T(1024)S(1)} %reshape.18), kind=kOutput, calls=%fused_computation.1 | convolution fusion | flops 4302307328 | bytes 16785408 | tf_op jit(solution)/shard_map/dot_general | solution.py:31
  172.7 0.0 copy-done
  172.7 6.8 %convolution_convert_fusion = bf16[2048,2048]{1,0:T(8,128)(2,1)} fusion(bf16[2048,512]{1,0:T(8,128)(2,1)S(1)} %multiply_convert_fusion, bf16[1,512,2048]{2,1,0:T(8,128)(2,1)S(1)} %copy-done), kind=kOutput, calls=%fused_computation | convolution fusion | flops 4299161600 | bytes 12582912 | tf_op jit(solution)/shard_map/dot_general | solution.py:34
  179.5 0.0 copy-start.1
  179.5 0.1 reduce-scatter.2.cloned.1.call-update
  179.5 0.8 copy-done.1
  180.4 2.0 fusion.16
  182.4 209.0 %reduce-scatter.2.cloned.1.call-done = bf16[32,2048]{1,0:T(8,128)(2,1)} async-done(((bf16[2048,2048]{1,0:T(8,128)(2,1)}), bf16[32,2048]{1,0:T(8,128)(2,1)}) %reduce-scatter.2.cloned.1.call-update) | async-done | bytes 131088 | tf_op jit(solution)/shard_map/reduce_scatter | solution.py:37
  391.4 3.8 fusion
  (1 shorter events, 0.0 us)
Async XLA Ops:
  6.5 166.1 %copy-start = (bf16[1,512,2048]{2,1,0:T(8,128)(2,1)S(1)}, bf16[1,512,2048]{2,1,0:T(8,128)(2,1)}, u32[]{:S(2)}) copy-start(bf16[1,512,2048]{2,1,0:T(8,128)(2,1)} %param.16) | copy-start | bytes 6291460
  6.6 153.2 %all-gather.4.cloned.1.call-start = ((), (), s32[]{:S(2)}) async-start(), calls=%async_computation.1 | async-start | bytes 8519680 | tf_op jit(solution)/shard_map/all_gather | solution.py:24
  9.5 381.9 %reduce-scatter.2.cloned.1.call-start = ((), (), s32[]{:S(2)}) async-start(), calls=%async_computation.2 | async-start | bytes 8519680 | tf_op jit(solution)/shard_map/reduce_scatter | solution.py:37
  159.7 7.7 %copy-start.2 = (bf16[2048,2048]{1,0:T(8,128)(2,1)S(1)}, bf16[2048,2048]{1,0:T(8,128)(2,1)}, u32[]{:S(2)}) copy-start(bf16[2048,2048]{1,0:T(8,128)(2,1)} %all-gather.4.cloned.1.call-done) | copy-start | bytes 25165828
  159.7 7.7 %copy-start.3 = (bf16[1,2048,512]{2,1,0:T(8,128)(2,1)S(1)}, bf16[1,2048,512]{2,1,0:T(8,128)(2,1)}, u32[]{:S(2)}) copy-start(bf16[1,2048,512]{2,1,0:T(8,128)(2,1)} %param.15) | copy-start | bytes 6291460
  179.5 0.9 copy-start.1
Sparse Core Ops, SparseCore 0:
  9.6 150.0 all-gather.3
  179.6 211.6 reduce-scatter.1
where the time goes:
time: 402 us
  waiting for transfers between devices  230 us (57%)
  blocking collectives  129 us (32%)
  matrix products  25.5 us (6%)
  between operations  13.5 us (3%)
    reduce_scatter x1, waiting for transfers between devices, body(): routed = lax.psum_scatter(part, 'ep', scatter_dimension=0, tiled=True)  209 us
    all_gather x1, blocking collectives, body(): routes = lax.all_gather(routing, 'ep', axis=0, tiled=True)  76.1 us
    all_gather x1, blocking collectives, body(): weights = lax.all_gather(gates, 'ep', axis=0, tiled=True)  53.4 us
    all_gather x1, waiting for transfers between devices, body(): everyone = lax.all_gather(normed, 'ep', axis=0, tiled=True)  20.5 us
  transfers between devices with their start and end apart: 2, of which 2 were waited for; matrix products, arithmetic and copies ran while one was open for 1% of the time, Pallas kernels for 0%

commit v1 on v0

--- a/solution.py
+++ b/solution.py
@@ -21,7 +21,11 @@
         * jnp.dot(normed, shared_up, preferred_element_type=jnp.float32)
     ).astype(jnp.bfloat16)
     shared_out = jnp.dot(shared_hidden, shared_down, preferred_element_type=jnp.float32)
-    everyone = lax.all_gather(normed, "ep", axis=0, tiled=True)
+    length = lax.axis_size("ep")
+    repeats = [length if d == 0 else 1 for d in range(normed.ndim)]
+    everyone = lax.all_to_all(
+        jnp.tile(normed, repeats), "ep", split_axis=0, concat_axis=0, tiled=True
+    )
     routes = lax.all_gather(routing, "ep", axis=0, tiled=True)
     weights = lax.all_gather(gates, "ep", axis=0, tiled=True)
     own = lax.axis_index("ep")

time: 402 us -> 1130 us (2.81)
  blocking collectives: 129 us -> 827 us
  starting transfers between devices: 0.07 us -> 34.5 us
  waiting for transfers between devices: 230 us -> 214 us
    all_gather x1, blocking collectives: 76.1 us -> 771 us  [body(): routes = lax.all_gather(routing, 'ep', axis=0, tiled=True)]
    all_to_all x0 -> x1, starting transfers between devices: none -> 34.4 us  [body(): lax.all_to_all(jnp.tile(normed, repeats), 'ep', split_axis=0, concat_axis...]
    all_gather x1 -> x0, waiting for transfers between devices: 20.5 us -> none  [body(): everyone = lax.all_gather(normed, 'ep', axis=0, tiled=True)]
  transfers between devices with their start and end apart: 2 -> 2, of which waited for: 2 -> 1; matrix products, arithmetic and copies ran while one was open for 1% -> 0% of each run, Pallas kernels for 0% -> 0%
where the time goes in v1:
time: 1130 us; the launch traced here: 1120 us
  blocking collectives  827 us (73%)
  waiting for transfers between devices  214 us (19%)
  starting transfers between devices  34.5 us (3%)
  matrix products  29.1 us (3%)
  between operations  13.5 us (1%)
    all_gather x1, blocking collectives, body(): routes = lax.all_gather(routing, 'ep', axis=0, tiled=True)  771 us
    reduce_scatter x1, waiting for transfers between devices, body(): routed = lax.psum_scatter(part, 'ep', scatter_dimension=0, tiled=True)  214 us
    all_gather x1, blocking collectives, body(): weights = lax.all_gather(gates, 'ep', axis=0, tiled=True)  55.5 us
    all_to_all x1, starting transfers between devices, body(): lax.all_to_all(jnp.tile(normed, repeats), 'ep', split_axis=0, concat_axis...  34.4 us
  transfers between devices with their start and end apart: 2, of which 1 were waited for; matrix products, arithmetic and copies ran while one was open for 0% of the time, Pallas kernels for 0%

profile of v1, /device:TPU:38, one launch (start us, length us, event | category | flops | bytes accessed | tf_op | source)
XLA Modules:
  0.0 1125.0 jit_solution(9212282284365409099)
XLA Ops:
  6.5 0.0 copy-start
  6.6 1.2 fusion.6
  7.7 1.0 fusion.8
  8.8 4.3 tile.2
  13.0 0.0 copy-start.1
  13.0 0.0 copy-start.2
  13.0 34.4 %all-to-all-start = ((bf16[64,32,2048]{2,1,0:T(8,128)(2,1)}), bf16[64,32,2048]{2,1,0:T(8,128)(2,1)}, u32[]{:S(2)}, u32[]{:S(2)}) async-start(bf16[64,32,2048]{2,1,0:T(8,128)(2,1)} %tile.2), calls=%async_computation | async-start | bytes 16777216 | tf_op jit(solution)/shard_map/all_to_all | solution.py:26
  47.4 0.1 reduce-scatter.2.cloned.1.call-start
  47.5 0.0 copy-done.1
  47.5 771.4 %all-gather = s32[64,32,8]{1,2,0:T(8,128)S(1)} all-gather(s32[1,32,8]{1,2,0:T(8,128)S(1)} %bitcast.20), channel_id=1, replica_groups=mesh['grp'=4,'ep'=64] {'ep'}, dimensions={0}, use_global_device_ids=true | all-gather | bytes 66560 | tf_op jit(solution)/shard_map/all_gather | solution.py:29
  819.0 0.0 copy-done.2
  819.0 55.5 %all-gather.1 = f32[64,32,8]{1,2,0:T(8,128)S(1)} all-gather(f32[1,32,8]{1,2,0:T(8,128)S(1)} %bitcast.21), channel_id=1, replica_groups=mesh['grp'=4,'ep'=64] {'ep'}, dimensions={0}, use_global_device_ids=true | all-gather | bytes 66560 | tf_op jit(solution)/shard_map/all_gather | solution.py:30
  874.4 0.1 select_reduce_fusion
  874.5 0.1 reshape.25
  874.6 0.0 all-to-all-done
  874.6 0.0 copy-start.3
  874.6 7.7 fusion.3
  882.3 0.0 copy-done.3
  882.3 8.9 multiply_convert_fusion
  891.2 0.0 copy-done
  891.2 6.7 convolution_convert_fusion
  898.0 0.1 reduce-scatter.2.cloned.1.call-update
  898.0 2.0 fusion.16
  900.1 214.3 %reduce-scatter.2.cloned.1.call-done = bf16[32,2048]{1,0:T(8,128)(2,1)} async-done(((bf16[2048,2048]{1,0:T(8,128)(2,1)}), bf16[32,2048]{1,0:T(8,128)(2,1)}) %reduce-scatter.2.cloned.1.call-update) | async-done | bytes 131088 | tf_op jit(solution)/shard_map/reduce_scatter | solution.py:41
  1114.3 3.8 fusion
  (1 shorter events, 0.0 us)
Async XLA Ops:
  6.5 884.7 %copy-start = (bf16[1,512,2048]{2,1,0:T(8,128)(2,1)S(1)}, bf16[1,512,2048]{2,1,0:T(8,128)(2,1)}, u32[]{:S(2)}) copy-start(bf16[1,512,2048]{2,1,0:T(8,128)(2,1)} %param.16) | copy-start | bytes 6291460
  13.0 34.5 %copy-start.1 = (s32[32,8]{0,1:T(8,128)S(1)}, s32[32,8]{0,1:T(8,128)}, u32[]{:S(2)}) copy-start(s32[32,8]{0,1:T(8,128)} %param.12) | copy-start | bytes 3076
  13.0 805.9 %copy-start.2 = (f32[32,8]{0,1:T(8,128)S(1)}, f32[32,8]{0,1:T(8,128)}, u32[]{:S(2)}) copy-start(f32[32,8]{0,1:T(8,128)} %param.13) | copy-start | bytes 3076
  13.0 861.6 %all-to-all-start = ((bf16[64,32,2048]{2,1,0:T(8,128)(2,1)}), bf16[64,32,2048]{2,1,0:T(8,128)(2,1)}, u32[]{:S(2)}, u32[]{:S(2)}) async-start(bf16[64,32,2048]{2,1,0:T(8,128)(2,1)} %tile.2), calls=%async_computation | async-start | bytes 16777216 | tf_op jit(solution)/shard_map/all_to_all | solution.py:26
  47.4 1066.9 %reduce-scatter.2.cloned.1.call-start = ((), (), s32[]{:S(2)}) async-start(), calls=%async_computation.2 | async-start | bytes 8519680 | tf_op jit(solution)/shard_map/reduce_scatter | solution.py:41
  874.6 7.7 copy-start.3
Sparse Core Ops, SparseCore 0:
  898.1 216.1 reduce-scatter.1
